TPU v7x, 32 devices: a whole 2x2x4 slice. The times are simulated.
32 devices in a mesh: sp: 8 (over z, y), tp: 4 (over x, core).
Axes of the slice: x: 2, y: 2, z: 4, core: 2. Of those that a mesh axis runs over, the one named last changes fastest.
Arguments:
- grad_out: bfloat16 [2048, 2048], P('sp'), may hold values from -6 to 6
- resid: bfloat16 [2048, 2048], P('sp'), may hold values from -6 to 6
- norm_gain: float32 [2048], replicated, may hold values from 0.1 to 1.9
- routes: int32 [2048, 2], P('sp'), may hold values from 0 to 7, all different within a row; in each aligned block of 256 rows (0 to 255, 256 to 511, ...) at most 96 rows name the same one
- route_weights: float32 [2048, 2], P('sp'), may hold values from 0.05 to 1
- gate_weight: bfloat16 [8, 2048, 1536], P('sp', None, 'tp'), may hold values from -0.375 to 0.375
- up_weight: bfloat16 [8, 2048, 1536], P('sp', None, 'tp'), may hold values from -0.375 to 0.375
- down_weight: bfloat16 [8, 1536, 2048], P('sp', 'tp'), may hold values from -0.15625 to 0.15625
- proj_weight: bfloat16 [2048, 512], P(None, 'tp'), may hold values from -0.25 to 0.25
- conv_sum: bfloat16 [2048, 512], P('sp', 'tp'), may hold values from -6 to 6
- conv_gain: float32 [512], P('tp'), may hold values from 0.1 to 1.9
- conv_taps: float32 [31, 512], P(None, 'tp'), may hold values from -1 to 1
- conv_value: bfloat16 [2048, 512], P('sp', 'tp'), may hold values from -6 to 6
- conv_gate: bfloat16 [2048, 512], P('sp', 'tp'), may hold values from -6 to 6
Outputs:
- gate_weight_grad: bfloat16 [8, 2048, 1536], P('sp', None, 'tp')
- up_weight_grad: bfloat16 [8, 2048, 1536], P('sp', None, 'tp')
- down_weight_grad: bfloat16 [8, 1536, 2048], P('sp', 'tp')
- proj_grad: float32 [2048, 512], P('sp', 'tp')
- value_grad: bfloat16 [2048, 512], P('sp', 'tp')
- gate_input_grad: bfloat16 [2048, 512], P('sp', 'tp')
Inputs may be any that keep to these rules, and one draw needn't show every extreme that they name: In each aligned block of 256 tokens no expert is named by more than 96 routes, and in some block one expert is named exactly 96 times; a token's two routes name different experts.
All inputs are finite; a program needn't handle non-finite values.
Results may differ from a plain program's by a relative error of at most 0.028.
Values may be sent and summed in bfloat16 or wider, within the bound.
A program may use at most 128 MiB of HBM per device.

v0:
```python
import jax
import jax.numpy as jnp
from jax import lax
from jax.sharding import PartitionSpec as P

CONV_K = 31
GROUP = 128


CLAMP_LIMIT = 7.0
SLOPE_ALPHA = 1.702


def passed_along(block, axis, distance):
    devices = range(lax.axis_size(axis))
    route = [(i - distance, i) for i in devices if i - distance in devices]
    return lax.ppermute(block, axis, route)


def contract_rows(left_side, right_side):
    return lax.dot_general(
        left_side, right_side, (((0,), (0,)), ((), ())), preferred_element_type=jnp.float32
    )


def contract_cols(left_side, right_side):
    return lax.dot_general(
        left_side, right_side, (((1,), (1,)), ((), ())), preferred_element_type=jnp.float32
    )


def expert_backward(routed_rows, routed_cots, w_gate, w_up, w_down):
    gate_pre = jnp.dot(routed_rows, w_gate, preferred_element_type=jnp.float32)
    up_pre = jnp.dot(routed_rows, w_up, preferred_element_type=jnp.float32)
    gate_clamped = jnp.minimum(gate_pre, CLAMP_LIMIT)
    up_clamped = jnp.clip(up_pre, -CLAMP_LIMIT, CLAMP_LIMIT)
    sigma = jax.nn.sigmoid(SLOPE_ALPHA * gate_clamped)
    gated = gate_clamped * sigma
    act = ((up_clamped + 1.0) * gated).astype(jnp.bfloat16)
    down_grad = contract_rows(act, routed_cots).astype(jnp.bfloat16)
    act_grad = contract_cols(routed_cots, w_down)
    inside = (up_pre > -CLAMP_LIMIT) & (up_pre < CLAMP_LIMIT)
    up_pre_grad = jnp.where(inside, act_grad * gated, 0.0).astype(jnp.bfloat16)
    slope = sigma + SLOPE_ALPHA * gate_clamped * sigma * (1.0 - sigma)
    gate_pre_grad = jnp.where(
        gate_pre < CLAMP_LIMIT, act_grad * (up_clamped + 1.0) * slope, 0.0
    ).astype(jnp.bfloat16)
    gate_grad = contract_rows(routed_rows, gate_pre_grad).astype(jnp.bfloat16)
    up_grad = contract_rows(routed_rows, up_pre_grad).astype(jnp.bfloat16)
    partial_value = contract_cols(gate_pre_grad, w_gate) + contract_cols(up_pre_grad, w_up)
    return (gate_grad, up_grad, down_grad, partial_value)


def local(
    grad_out,
    resid,
    norm_gain,
    routes,
    route_weights,
    gate_weight,
    up_weight,
    down_weight,
    proj_weight,
    conv_sum,
    conv_gain,
    conv_taps,
    conv_value,
    conv_gate,
):
    tok_rows, model_width = resid.shape
    sp_count = lax.axis_size("sp")
    tp_count = lax.axis_size("tp")
    capacity = 3 * tok_rows // sp_count
    col_count = model_width // tp_count
    resid_f = resid.astype(jnp.float32)
    inv_rms = lax.rsqrt(jnp.mean(resid_f * resid_f, axis=-1, keepdims=True) + 1e-06)
    normed = (resid_f * inv_rms * norm_gain).astype(jnp.bfloat16)
    scaled = (route_weights[:, :, None] * grad_out.astype(jnp.float32)[:, None, :]).astype(
        jnp.bfloat16
    )
    scaled = scaled.reshape(2 * tok_rows, model_width)
    route_ids = routes.reshape(-1)
    one_hot = (route_ids[:, None] == jnp.arange(sp_count, dtype=jnp.int32)[None, :]).astype(
        jnp.int32
    )
    slot_rank = jnp.sum(jnp.cumsum(one_hot, axis=0) * one_hot, axis=1) - 1
    slot_index = route_ids * capacity + slot_rank
    slot_table = jnp.full((sp_count * capacity,), 2 * tok_rows, jnp.int32)
    slot_table = slot_table.at[slot_index].set(jnp.arange(2 * tok_rows, dtype=jnp.int32))
    normed_pad = jnp.concatenate([normed, jnp.zeros((1, model_width), jnp.bfloat16)], axis=0)
    scaled_pad = jnp.concatenate([scaled, jnp.zeros((1, model_width), jnp.bfloat16)], axis=0)
    first_col = lax.axis_index("tp") * col_count
    normed_part = lax.dynamic_slice_in_dim(normed_pad, first_col, col_count, 1)
    scaled_part = lax.dynamic_slice_in_dim(scaled_pad, first_col, col_count, 1)
    send_rows = normed_part[slot_table // 2].reshape(sp_count, capacity, col_count)
    send_cots = scaled_part[slot_table].reshape(sp_count, capacity, col_count)
    part_rows, part_cots = (
        lax.all_to_all(send_rows, "sp", split_axis=0, concat_axis=0, tiled=True),
        lax.all_to_all(send_cots, "sp", split_axis=0, concat_axis=0, tiled=True),
    )
    routed_rows, routed_cots = (
        lax.all_gather(part_rows, "tp", axis=2, tiled=True),
        lax.all_gather(part_cots, "tp", axis=2, tiled=True),
    )
    routed_rows = routed_rows.reshape(sp_count * capacity, model_width)
    routed_cots = routed_cots.reshape(sp_count * capacity, model_width)
    gate_grad, up_grad, down_grad, partial_value = expert_backward(
        routed_rows, routed_cots, gate_weight[0], up_weight[0], down_weight[0]
    )
    row_grad = lax.psum_scatter(
        partial_value.reshape(sp_count, capacity, model_width).astype(jnp.bfloat16),
        "tp",
        scatter_dimension=2,
        tiled=True,
    )
    returned = lax.all_to_all(row_grad, "sp", split_axis=0, concat_axis=0, tiled=True).reshape(
        sp_count * capacity, col_count
    )
    normed_part_grad = returned[slot_index].reshape(tok_rows, 2, col_count).astype(jnp.float32)
    normed_part_grad = normed_part_grad.sum(axis=1).astype(jnp.bfloat16)
    normed_grad = lax.all_gather(normed_part_grad, "tp", axis=1, tiled=True)
    feature_grad = normed_grad.astype(jnp.float32) * norm_gain
    cubed = inv_rms * inv_rms * inv_rms
    resid_grad = (
        grad_out.astype(jnp.float32)
        + inv_rms * feature_grad
        - resid_f * cubed * jnp.mean(resid_f * feature_grad, axis=-1, keepdims=True)
    ).astype(jnp.bfloat16)
    channels = conv_sum.shape[1]
    summed = conv_sum.astype(jnp.float32).reshape(tok_rows, channels // GROUP, GROUP)
    centre = summed - jnp.mean(summed, axis=-1, keepdims=True)
    inv_std = lax.rsqrt(jnp.mean(centre * centre, axis=-1, keepdims=True) + 1e-05)
    grouped = centre * inv_std
    chan_normed = grouped.reshape(tok_rows, channels)
    pre_act = chan_normed * conv_gain
    sigma_conv = jax.nn.sigmoid(pre_act)
    conv_out = (pre_act * sigma_conv).astype(jnp.bfloat16)
    proj_grad = lax.psum_scatter(
        contract_rows(resid_grad, conv_out), "sp", scatter_dimension=0, tiled=True
    )
    out_grad = jnp.dot(resid_grad, proj_weight, preferred_element_type=jnp.float32)
    normal_grad = (
        out_grad * sigma_conv * (1.0 + pre_act * (1.0 - sigma_conv)) * conv_gain
    ).reshape(tok_rows, channels // GROUP, GROUP)
    sum_grad = inv_std * (
        normal_grad
        - jnp.mean(normal_grad, axis=-1, keepdims=True)
        - grouped * jnp.mean(normal_grad * grouped, axis=-1, keepdims=True)
    )
    sum_grad = sum_grad.reshape(tok_rows, channels)
    following = passed_along(sum_grad[: CONV_K - 1], "sp", -1)
    extended = jnp.concatenate([sum_grad, following], axis=0)
    gated_grad = lax.conv_general_dilated(
        extended[None],
        conv_taps[::-1][:, None, :],
        (1,),
        ((0, 0),),
        dimension_numbers=("NWC", "WIO", "NWC"),
        feature_group_count=channels,
        precision=lax.Precision.HIGHEST,
    )[0]
    sigma_gate = jax.nn.sigmoid(conv_gate.astype(jnp.float32))
    value_grad = (gated_grad * sigma_gate).astype(jnp.bfloat16)
    gate_input_grad = (
        gated_grad * conv_value.astype(jnp.float32) * sigma_gate * (1.0 - sigma_gate)
    ).astype(jnp.bfloat16)
    return (gate_grad[None], up_grad[None], down_grad[None], proj_grad, value_grad, gate_input_grad)


def solution(mesh):
    in_specs = (
        P("sp", None),
        P("sp", None),
        P(),
        P("sp", None),
        P("sp", None),
        P("sp", None, "tp"),
        P("sp", None, "tp"),
        P("sp", "tp", None),
        P(None, "tp"),
        P("sp", "tp"),
        P("tp"),
        P(None, "tp"),
        P("sp", "tp"),
        P("sp", "tp"),
    )
    out_specs = (
        P("sp", None, "tp"),
        P("sp", None, "tp"),
        P("sp", "tp", None),
        P("sp", "tp"),
        P("sp", "tp"),
        P("sp", "tp"),
    )
    return jax.shard_map(local, mesh=mesh, in_specs=in_specs, out_specs=out_specs, check_vma=False)
```

profile of v0, /device:TPU:0, one launch (start us, length us, event | category | flops | bytes accessed | tf_op | source)
XLA Modules:
  0.0 286.5 jit_solution(7567787872542346004)
XLA Ops:
  7.2 0.0 all-gather.4.cloned.1.call-start
  7.3 0.8 broadcast_multiply_fusion
  8.1 0.8 copy.25
  8.9 0.1 eq.29
  9.1 0.1 eq.25
  9.2 1.5 fusion.3
  10.7 0.1 copy.24
  10.9 0.1 mul.210
  11.0 1.1 reduce-window.6
  12.2 0.2 slice_reduce_fusion
  12.4 0.1 fusion.53
  12.6 2.4 scatter_custom_fusion
  15.0 0.3 fusion.5
  15.4 3.3 %gather_fusion = bf16[768,512]{1,0:T(8,128)(2,1)} fusion(bf16[257,512]{1,0:T(8,128)(2,1)S(1)} %pad_dynamic-slice_fusion.1, s32[1024]{0:T(1024)S(1)} %get-tuple-element.18), kind=kCustom, calls=%fused_computation | custom fusion | bytes 1575936 | tf_op jit(solution)/shard_map/gather | solution.py:95
  18.7 27.6 %all_to_all.15 = bf16[8,96,512]{2,1,0:T(8,128)(2,1)} all-to-all(bf16[8,96,512]{2,1,0:T(8,128)(2,1)} %bitcast.63), channel_id=1, replica_groups=mesh['sp'=8,'tp'=4] {'sp'}, dimensions={0} | all-to-all | bytes 1572864 | tf_op jit(solution)/shard_map/all_to_all | solution.py:98
  46.3 0.0 all-gather.4.cloned.1.call-update
  46.3 0.0 all-gather.6.cloned.1.call-start
  46.4 5.3 %mul.214 = f32[256,2,2048]{2,1,0:T(2,128)} broadcast(bf16[256,2048]{1,0:T(8,128)(2,1)} %param.14), dimensions={0,2} | broadcast | bytes 5242880 | tf_op jit(solution)/shard_map/mul | solution.py:78
  51.7 6.2 %mul.215 = f32[512,2048]{1,0:T(8,128)} reshape(f32[256,2,2048]{2,1,0:T(2,128)} %mul.214) | data formatting | bytes 8388608 | tf_op jit(solution)/shard_map/mul | solution.py:78
  57.8 0.1 copy.27
  58.0 0.1 mul.212
  58.1 2.5 multiply_convert_fusion
  60.7 3.3 %gather_fusion.1 = bf16[768,512]{1,0:T(8,128)(2,1)} fusion(bf16[513,512]{1,0:T(8,128)(2,1)S(1)} %pad_dynamic-slice_fusion, s32[1024]{0:T(1024)S(1)} %get-tuple-element.17), kind=kCustom, calls=%fused_computation.1 | custom fusion | bytes 1575936 | tf_op jit(solution)/shard_map/gather | solution.py:96
  64.0 23.7 %all_to_all.16 = bf16[8,96,512]{2,1,0:T(8,128)(2,1)} all-to-all(bf16[8,96,512]{2,1,0:T(8,128)(2,1)} %bitcast.64), channel_id=1, replica_groups=mesh['sp'=8,'tp'=4] {'sp'}, dimensions={0} | all-to-all | bytes 1572864 | tf_op jit(solution)/shard_map/all_to_all | solution.py:99
  87.7 0.0 all-gather.6.cloned.1.call-update
  87.7 0.2 reduce-scatter.3.cloned.1.call-start
  87.9 0.0 all-gather.4.cloned.1.call-done
  88.0 5.3 %fusion.11 = f32[768,384]{1,0:T(8,128)} fusion(bf16[768,2048]{1,0:T(8,128)(2,1)} %bitcast.70, bf16[1,2048,384]{2,1,0:T(8,128)(2,1)} %param.20), kind=kOutput, calls=%fused_computation.26 | convolution fusion | flops 1207959552 | bytes 5898240 | tf_op jit(solution)/shard_map/dot_general | solution.py:34
  93.3 2.8 fusion.17
  96.1 19.2 %all-gather.6.cloned.1.call-done = bf16[8,96,2048]{2,1,0:T(8,128)(2,1)} async-done(((bf16[8,96,512]{2,1,0:T(8,128)(2,1)}), bf16[8,96,2048]{2,1,0:T(8,128)(2,1)}) %all-gather.6.cloned.1.call-update) | async-done | bytes 3145744 | tf_op jit(solution)/shard_map/all_gather | solution.py:103
  115.3 5.5 %select_convert_fusion = (bf16[768,384]{1,0:T(8,128)(2,1)S(1)}, bf16[768,384]{1,0:T(8,128)(2,1)S(1)}) fusion(f32[768,384]{1,0:T(8,128)} %fusion.11, f32[768,384]{1,0:T(8,128)} %fusion.17, bf16[768,2048]{1,0:T(8,128)(2,1)} %bitcast.74, bf16[1,384,2048]{2,1,0:T(8,128)(2,1)} %param.21), kind=kOutput, calls=%fused_computation.35 | convolution fusion | flops 1214742528 | bytes 8257536 | tf_op jit(solution)/shard_map/dot_general | solution.py:27
  120.8 1.8 fusion.15
  122.7 3.5 %add_convert_fusion = bf16[768,2048]{1,0:T(8,128)(2,1)} fusion(f32[768,2048]{1,0:T(8,128)S(1)} %fusion.15, bf16[768,384]{1,0:T(8,128)(2,1)S(1)} %get-tuple-element.8, bf16[1,2048,384]{2,1,0:T(8,128)(2,1)S(1)} %copy-done.6), kind=kOutput, calls=%fused_computation.4 | convolution fusion | flops 1211105280 | bytes 11599872 | tf_op jit(solution)/shard_map/dot_general | solution.py:27
  126.2 0.0 reduce-scatter.3.cloned.1.call-update
  126.2 37.9 %reduce-scatter.3.cloned.1.call-done = bf16[8,96,512]{2,1,0:T(8,128)(2,1)} async-done(((bf16[8,96,2048]{2,1,0:T(8,128)(2,1)}), bf16[8,96,512]{2,1,0:T(8,128)(2,1)}) %reduce-scatter.3.cloned.1.call-update) | async-done | bytes 786448 | tf_op jit(solution)/shard_map/reduce_scatter | solution.py:110
  164.1 5.5 %all-to-all-start.2 = ((bf16[8,96,512]{2,1,0:T(8,128)(2,1)}), bf16[8,96,512]{2,1,0:T(8,128)(2,1)S(1)}, u32[]{:S(2)}, u32[]{:S(2)}) async-start(bf16[8,96,512]{2,1,0:T(8,128)(2,1)} %reduce-scatter.3.cloned.1.call-done), calls=%async_computation.3 | async-start | bytes 1572864 | tf_op jit(solution)/shard_map/all_to_all | solution.py:116
  169.6 0.0 all-gather.8.cloned.1.call-start
  169.6 20.0 %all-to-all-done.2 = bf16[8,96,512]{2,1,0:T(8,128)(2,1)S(1)} async-done(((bf16[8,96,512]{2,1,0:T(8,128)(2,1)}), bf16[8,96,512]{2,1,0:T(8,128)(2,1)S(1)}, u32[]{:S(2)}, u32[]{:S(2)}) %all-to-all-start.2) | async-done | bytes 786464 | tf_op jit(solution)/shard_map/all_to_all | solution.py:116
  189.6 2.6 gather_fusion.2
  192.3 1.3 reshape.172
  193.5 2.1 reduce_sum.77
  195.6 0.0 all-gather.8.cloned.1.call-update
  195.7 0.3 reduce-scatter.5.cloned.1.call-start
  196.0 0.1 convert_reduce_fusion
  196.1 0.2 fusion.46
  196.3 5.3 %fusion.2 = bf16[1,384,2048]{2,1,0:T(8,128)(2,1)} fusion(bf16[768,2048]{1,0:T(8,128)(2,1)} %bitcast.75, f32[768,384]{1,0:T(8,128)} %fusion.11, f32[768,384]{1,0:T(8,128)} %fusion.17), kind=kOutput, calls=%fused_computation.15 | convolution fusion | flops 1211695104 | bytes 7077888 | tf_op jit(solution)/shard_map/dot_general | solution.py:21
  201.6 8.9 %all-gather.8.cloned.1.call-done = bf16[256,2048]{1,0:T(8,128)(2,1)} async-done(((bf16[256,512]{1,0:T(8,128)(2,1)}), bf16[256,2048]{1,0:T(8,128)(2,1)}) %all-gather.8.cloned.1.call-update) | async-done | bytes 1048592 | tf_op jit(solution)/shard_map/all_gather | solution.py:121
  210.5 1.8 fusion.9
  212.3 0.0 copy-done.5
  212.3 0.7 fusion.8
  213.1 1.0 copy-done.3
  214.0 1.5 fusion.47
  215.6 0.0 reduce-scatter.5.cloned.1.call-update
  215.6 5.1 %fusion = bf16[1,2048,384]{2,1,0:T(8,128)(2,1)} fusion(bf16[768,2048]{1,0:T(8,128)(2,1)} %bitcast.71, bf16[768,384]{1,0:T(8,128)(2,1)} %copy-done.8), kind=kOutput, calls=%fused_computation.13 | convolution fusion | flops 1208745984 | bytes 5308416 | tf_op jit(solution)/shard_map/dot_general | solution.py:21
  220.8 0.6 fusion.67
  221.3 0.2 fusion.45
  221.6 1.3 collective-permute-start
  222.9 3.0 %fusion.1 = bf16[1,2048,384]{2,1,0:T(8,128)(2,1)} fusion(bf16[768,2048]{1,0:T(8,128)(2,1)S(1)} %bitcast.73, bf16[768,384]{1,0:T(8,128)(2,1)S(1)} %copy-done.10), kind=kOutput, calls=%fused_computation.14 | convolution fusion | flops 1208745984 | bytes 5308416 | tf_op jit(solution)/shard_map/dot_general | solution.py:21
  225.9 1.3 collective-permute-done
  227.3 0.3 convolution_select_fusion
  227.7 0.4 copy-done.12
  228.1 0.0 copy-done.13
  228.2 0.7 multiply_convert_fusion.3
  228.9 51.1 %reduce-scatter.5.cloned.1.call-done = f32[256,128]{1,0:T(8,128)} async-done(((f32[2048,128]{1,0:T(8,128)}), f32[256,128]{1,0:T(8,128)}) %reduce-scatter.5.cloned.1.call-update) | async-done | bytes 131088 | tf_op jit(solution)/shard_map/reduce_scatter | solution.py:138
  (63 shorter events, 0.4 us)
Async XLA Ops:
  7.2 86.1 %copy-start = (bf16[1,2048,384]{2,1,0:T(8,128)(2,1)S(1)}, bf16[1,2048,384]{2,1,0:T(8,128)(2,1)}, u32[]{:S(2)}) copy-start(bf16[1,2048,384]{2,1,0:T(8,128)(2,1)} %param.19) | copy-start | bytes 4718596
  7.2 7.8 %copy-start.1 = (bf16[256,2048]{1,0:T(8,128)(2,1)S(1)}, bf16[256,2048]{1,0:T(8,128)(2,1)}, u32[]{:S(2)}) copy-start(bf16[256,2048]{1,0:T(8,128)(2,1)} %param.15) | copy-start | bytes 3145732
  7.2 7.8 %copy-start.11 = (f32[2048]{0:T(1024)S(1)}, f32[2048]{0:T(1024)}, u32[]{:S(2)}) copy-start(f32[2048]{0:T(1024)} %param.16) | copy-start | bytes 24580
  7.2 80.8 %all-gather.4.cloned.1.call-start = ((), (), s32[]{:S(2)}) async-start(), calls=%async_computation.5 | async-start | bytes 3932160 | tf_op jit(solution)/shard_map/all_gather | solution.py:102
  46.3 69.0 %all-gather.6.cloned.1.call-start = ((), (), s32[]{:S(2)}) async-start(), calls=%async_computation.6 | async-start | bytes 3932160 | tf_op jit(solution)/shard_map/all_gather | solution.py:103
  51.7 6.2 %copy-start.15 = (f32[256,2]{0,1:T(2,128)S(1)}, f32[256,2]{0,1:T(2,128)}, u32[]{:S(2)}) copy-start(f32[256,2]{0,1:T(2,128)} %param.18) | copy-start | bytes 6148
  87.7 76.3 %reduce-scatter.3.cloned.1.call-start = ((), (), s32[]{:S(2)}) async-start(), calls=%async_computation.7 | async-start | bytes 3932160 | tf_op jit(solution)/shard_map/reduce_scatter | solution.py:110
  88.0 5.3 %copy-start.17 = (bf16[8,96,2048]{2,1,0:T(8,128)(2,1)S(1)}, bf16[8,96,2048]{2,1,0:T(8,128)(2,1)}, u32[]{:S(2)}) copy-start(bf16[8,96,2048]{2,1,0:T(8,128)(2,1)} %all-gather.4.cloned.1.call-done) | copy-start | bytes 9437188
  120.8 1.9 copy-start.8
  120.8 1.9 copy-start.9
  120.8 1.9 copy-start.6
  164.1 25.6 %all-to-all-start.2 = ((bf16[8,96,512]{2,1,0:T(8,128)(2,1)}), bf16[8,96,512]{2,1,0:T(8,128)(2,1)S(1)}, u32[]{:S(2)}, u32[]{:S(2)}) async-start(bf16[8,96,512]{2,1,0:T(8,128)(2,1)} %reduce-scatter.3.cloned.1.call-done), calls=%async_computation.3 | async-start | bytes 1572864 | tf_op jit(solution)/shard_map/all_to_all | solution.py:116
  169.6 40.9 %all-gather.8.cloned.1.call-start = ((), (), s32[]{:S(2)}) async-start(), calls=%async_computation.8 | async-start | bytes 1310720 | tf_op jit(solution)/shard_map/all_gather | solution.py:121
  192.3 3.7 %copy-start.14 = (f32[31,128]{1,0:T(8,128)S(1)}, f32[31,128]{1,0:T(8,128)}, u32[]{:S(2)}) copy-start(f32[31,128]{1,0:T(8,128)} %param.25) | copy-start | bytes 47620
  192.3 3.7 %copy-start.7 = (bf16[256,128]{1,0:T(8,128)(2,1)S(1)}, bf16[256,128]{1,0:T(8,128)(2,1)}, u32[]{:S(2)}) copy-start(bf16[256,128]{1,0:T(8,128)(2,1)} %param.23) | copy-start | bytes 196612
  195.7 84.3 %reduce-scatter.5.cloned.1.call-start = ((), (), s32[]{:S(2)}) async-start(), calls=%async_computation.9 | async-start | bytes 1179648 | tf_op jit(solution)/shard_map/reduce_scatter | solution.py:138
  210.5 1.8 copy-start.2
  210.5 1.9 copy-start.5
  212.3 1.7 copy-start.16
  213.1 1.0 copy-start.3
  215.6 5.2 %copy-start.4 = (bf16[256,2048]{1,0:T(8,128)(2,1)S(1)}, bf16[256,2048]{1,0:T(8,128)(2,1)}, u32[]{:S(2)}) copy-start(bf16[256,2048]{1,0:T(8,128)(2,1)} %copy-done.3) | copy-start | bytes 3145732
  215.6 5.2 %copy-start.19 = (bf16[2048,128]{1,0:T(8,128)(2,1)S(1)}, bf16[2048,128]{1,0:T(8,128)(2,1)}, u32[]{:S(2)}) copy-start(bf16[2048,128]{1,0:T(8,128)(2,1)} %param.22) | copy-start | bytes 1572868
  215.6 7.3 %copy-start.18 = (bf16[8,96,2048]{2,1,0:T(8,128)(2,1)S(1)}, bf16[8,96,2048]{2,1,0:T(8,128)(2,1)}, u32[]{:S(2)}) copy-start(bf16[8,96,2048]{2,1,0:T(8,128)(2,1)} %all-gather.4.cloned.1.call-done) | copy-start | bytes 9437188
  220.8 2.1 copy-start.10
  221.6 5.7 %copy-start.20 = (pred[8,36]{0,1:T(8,128)(4,1)S(1)}, pred[8,36]{0,1:T(8,128)(4,1)}, u32[]{:S(2)}) copy-start(pred[8,36]{0,1:T(8,128)(4,1)} %constant.83) | copy-start | bytes 868
  221.6 5.6 %collective-permute-start = (f32[30,128]{1,0:T(8,128)S(1)}, f32[30,128]{1,0:T(8,128)S(1)}, u32[]{:S(2)}, u32[]{:S(2)}) collective-permute-start(f32[30,128]{1,0:T(8,128)S(1)} %slice.23), channel_id=1, source_target_pairs={{4,0},{8,4},{12,8},{16,12},{20,16},{24,20},{28,24},{5,1},{9,5},{13... | collective-permute-start | bytes 46088 | tf_op jit(solution)/shard_map/ppermute | solution.py:17
  227.3 0.8 copy-start.12
  227.3 0.9 copy-start.13
Sparse Core Ops, SparseCore 0:
  46.4 27.4 all-gather.3
  87.8 27.3 all-gather.5
  126.3 37.7 reduce-scatter.2
  195.8 14.6 all-gather.7
  215.7 64.2 reduce-scatter.4
where the time goes:
time: 287 us; the launch traced here: 286 us
  waiting for transfers between devices  138 us (48%)
  blocking collectives  51.2 us (18%)
  matrix products  34.8 us (12%)
  local copies, waits for them, and re-layouts  28.1 us (10%)
  between operations  14.2 us (5%)
  other arithmetic  12.3 us (4%)
  starting transfers between devices  7.41 us (3%)
    reduce_scatter x1, waiting for transfers between devices, local(): lax.psum_scatter(contract_rows(resid_grad, conv_out), 'sp', scatter_dimen...  51.1 us
    reduce_scatter x1, waiting for transfers between devices, local(): lax.psum_scatter(partial_value.reshape(sp_count, capacity, model_width).a...  37.9 us
    all_to_all x1, blocking collectives, local(): lax.all_to_all(send_rows, 'sp', split_axis=0, concat_axis=0, tiled=True)  27.6 us
    all_to_all x1, blocking collectives, local(): lax.all_to_all(send_cots, 'sp', split_axis=0, concat_axis=0, tiled=True)  23.7 us
    all_to_all x1, waiting for transfers between devices, local(): lax.all_to_all(row_grad, 'sp', split_axis=0, concat_axis=0, tiled=True)  20 us
    all_gather x1, waiting for transfers between devices, local(): lax.all_gather(part_cots, 'tp', axis=2, tiled=True)  19.2 us
    dot_general x4, matrix products, contract_rows(): lax.dot_general(left_side, right_side, (((0,), (0,)), ((), ())), preferre...  15 us
    mul x3, local copies, waits for them, and re-layouts, local(): route_weights[:, :, None] * grad_out.astype(jnp.float32)[:, None, :]  11.6 us
  transfers between devices with their start and end apart: 7, of which 6 were waited for; matrix products, arithmetic and copies ran while one was open for 14% of the time, Pallas kernels for 0%

commit v1 on v0

--- a/solution.py
+++ b/solution.py
@@ -1,10 +1,15 @@
+import functools
+
 import jax
 import jax.numpy as jnp
 from jax import lax
+from jax.experimental import pallas as pl
+from jax.experimental.pallas import tpu as pltpu
 from jax.sharding import PartitionSpec as P
 
 CONV_K = 31
 GROUP = 128
+MESH = pl.DeviceIdType.MESH
 
 
 CLAMP_LIMIT = 7.0
@@ -15,6 +20,266 @@
     devices = range(lax.axis_size(axis))
     route = [(i - distance, i) for i in devices if i - distance in devices]
     return lax.ppermute(block, axis, route)
+
+
+def rotated(block, axis, distance):
+    count = lax.axis_size(axis)
+    return lax.ppermute(block, axis, [(i, (i + distance) % count) for i in range(count)])
+
+
+def tp_places():
+    mine = lax.axis_index("tp")
+    near = mine + 1 - 2 * (mine % 2)
+    far = (mine + 2) % 4
+    diag = (near + 2) % 4
+    return mine, near, far, diag
+
+
+def meet(steps, over_sp, near, far):
+    s, t = lax.axis_index("sp"), lax.axis_index("tp")
+    barrier = pltpu.get_barrier_semaphore()
+    pl.semaphore_signal(barrier, inc=1, device_id=(s, near), device_id_type=MESH)
+    pl.semaphore_signal(barrier, inc=1, device_id=(s, far), device_id_type=MESH)
+    total = 2
+    if over_sp:
+
+        def greet(d, carry):
+            pl.semaphore_signal(
+                barrier, inc=1, device_id=((s + d) % steps, t), device_id_type=MESH
+            )
+            return carry
+
+        lax.fori_loop(1, steps, greet, 0)
+        total += steps - 1
+    pl.semaphore_wait(barrier, total)
+
+
+def spread_kernel(count, steps, over_sp, in_lanes, absolute, *refs):
+    sends, outs = refs[:count], refs[count : 2 * count]
+    own_sem, a_send, a_recv, b_send, f_send, c_send, near_recv, fwd_recv, far_recv = refs[2 * count :]
+    s = lax.axis_index("sp")
+    t, near, far, _ = tp_places()
+    width = sends[0].shape[-1]
+
+    def place(c, d, q):
+        if in_lanes:
+            return outs[c].at[d, :, pl.ds(pl.multiple_of(q * width, width), width)]
+        return outs[c].at[d, q]
+
+    def source(c, d):
+        return sends[c].at[(s + d) % steps if absolute else d]
+
+    def own(c, d):
+        return pltpu.make_async_copy(source(c, d), place(c, d, t), own_sem.at[c, d])
+
+    def to_sp(c, d):
+        return pltpu.make_async_remote_copy(
+            src_ref=source(c, d),
+            dst_ref=place(c, d, t),
+            send_sem=a_send.at[c, d],
+            recv_sem=a_recv.at[c, d],
+            device_id=((s + d) % steps, t),
+            device_id_type=MESH,
+        )
+
+    def to_tp(c, d, q, target, send_sem, recv_sem):
+        return pltpu.make_async_remote_copy(
+            src_ref=place(c, d, q),
+            dst_ref=place(c, d, q),
+            send_sem=send_sem.at[c, d],
+            recv_sem=recv_sem.at[c, d],
+            device_id=(s, target),
+            device_id_type=MESH,
+        )
+
+    def near_copy(c, d):
+        return to_tp(c, d, t, near, b_send, near_recv)
+
+    def far_copy(c, d):
+        return to_tp(c, d, t, far, f_send, far_recv)
+
+    def fwd_copy(c, d):
+        return to_tp(c, d, far, near, c_send, fwd_recv)
+
+    def loop(first, last, body):
+        def step(d, carry):
+            for c in range(count):
+                body(c, d)
+            return carry
+
+        lax.fori_loop(first, last, step, 0)
+
+    meet(steps, over_sp, near, far)
+    remote_from = 1 if over_sp else steps
+    loop(0, remote_from, lambda c, d: own(c, d).start())
+    loop(remote_from, steps, lambda c, d: to_sp(c, d).start())
+
+    def share(c, d):
+        far_copy(c, d).start()
+        near_copy(c, d).start()
+
+    def forward(c, d):
+        far_copy(c, d).wait_recv()
+        fwd_copy(c, d).start()
+
+    def share_own(c, d):
+        own(c, d).wait()
+        share(c, d)
+
+    def share_arrived(c, d):
+        to_sp(c, d).wait_recv()
+        share(c, d)
+        forward(c, d - 1)
+
+    loop(0, remote_from, share_own)
+    loop(remote_from, steps, share_arrived)
+    loop(steps - 1 if over_sp else 0, steps, forward)
+
+    def finish(c, d):
+        near_copy(c, d).wait()
+        far_copy(c, d).wait_send()
+        fwd_copy(c, d).wait()
+
+    loop(0, steps, finish)
+    loop(remote_from, steps, lambda c, d: to_sp(c, d).wait_send())
+
+
+def spread(sends, over_sp, in_lanes, absolute, collective_id):
+    count = len(sends)
+    steps, rows, width = sends[0].shape
+    tp_count = lax.axis_size("tp")
+    shape = (steps, rows, tp_count * width) if in_lanes else (steps, tp_count, rows, width)
+    return pl.pallas_call(
+        functools.partial(spread_kernel, count, steps, over_sp, in_lanes, absolute),
+        out_shape=tuple(jax.ShapeDtypeStruct(shape, x.dtype) for x in sends),
+        in_specs=[pl.BlockSpec(memory_space=pltpu.VMEM)] * count,
+        out_specs=tuple(pl.BlockSpec(memory_space=pltpu.VMEM) for _ in sends),
+        scratch_shapes=[pltpu.SemaphoreType.DMA((count, steps))] * 9,
+        compiler_params=pltpu.CompilerParams(
+            collective_id=collective_id, has_side_effects=True, vmem_limit_bytes=40 << 20
+        ),
+    )(*sends)
+
+
+def combine_kernel(
+    steps, part, out, near_in, pair, far_in, total,
+    n0_send, n0_recv, n1_send, n1_recv, f_send, f_recv, a_send, a_recv,
+):
+    s = lax.axis_index("sp")
+    t, near, far, diag = tp_places()
+    width = out.shape[-1]
+
+    def lanes(q):
+        return pl.ds(pl.multiple_of(q * width, width), width)
+
+    def near_copy(d, which, q, send_sem, recv_sem):
+        return pltpu.make_async_remote_copy(
+            src_ref=part.at[d, :, lanes(q)],
+            dst_ref=near_in.at[which, d],
+            send_sem=send_sem.at[d],
+            recv_sem=recv_sem.at[d],
+            device_id=(s, near),
+            device_id_type=MESH,
+        )
+
+    def for_near(d):
+        return near_copy(d, 0, near, n0_send, n0_recv)
+
+    def for_diag(d):
+        return near_copy(d, 1, diag, n1_send, n1_recv)
+
+    def far_copy(d):
+        return pltpu.make_async_remote_copy(
+            src_ref=pair.at[d],
+            dst_ref=far_in.at[d],
+            send_sem=f_send.at[d],
+            recv_sem=f_recv.at[d],
+            device_id=(s, far),
+            device_id_type=MESH,
+        )
+
+    def back(d):
+        return pltpu.make_async_remote_copy(
+            src_ref=total.at[d],
+            dst_ref=out.at[d],
+            send_sem=a_send.at[d],
+            recv_sem=a_recv.at[d],
+            device_id=((s + steps - d) % steps, t),
+            device_id_type=MESH,
+        )
+
+    def loop(first, last, body):
+        def step(d, carry):
+            body(d)
+            return carry
+
+        lax.fori_loop(first, last, step, 0)
+
+    meet(steps, True, near, far)
+
+    def open_up(d):
+        for_diag(d).start()
+        for_near(d).start()
+
+    def add_pair(d):
+        for_diag(d).wait_recv()
+        mine = part[d, :, lanes(far)].astype(jnp.float32)
+        pair[d] = (mine + near_in[1, d].astype(jnp.float32)).astype(pair.dtype)
+        far_copy(d).start()
+
+    def whole(d):
+        for_near(d).wait_recv()
+        far_copy(d).wait_recv()
+        mine = part[d, :, lanes(t)].astype(jnp.float32)
+        both = mine + near_in[0, d].astype(jnp.float32)
+        return (both + far_in[d].astype(jnp.float32)).astype(out.dtype)
+
+    def send_back(d):
+        total[d] = whole(d)
+        back(d).start()
+
+    loop(1, steps, open_up)
+    open_up(0)
+    add_pair(1)
+
+    def middle(d):
+        add_pair(d)
+        send_back(d - 1)
+
+    loop(2, steps, middle)
+    add_pair(0)
+    send_back(steps - 1)
+    out[0] = whole(0)
+
+    def finish(d):
+        for_near(d).wait_send()
+        for_diag(d).wait_send()
+        far_copy(d).wait_send()
+
+    loop(0, steps, finish)
+    loop(1, steps, lambda d: back(d).wait())
+
+
+def combine(part, collective_id):
+    steps, rows, all_width = part.shape
+    width = all_width // lax.axis_size("tp")
+    block = (steps, rows, width)
+    return pl.pallas_call(
+        functools.partial(combine_kernel, steps),
+        out_shape=jax.ShapeDtypeStruct(block, part.dtype),
+        in_specs=[pl.BlockSpec(memory_space=pltpu.VMEM)],
+        out_specs=pl.BlockSpec(memory_space=pltpu.VMEM),
+        scratch_shapes=[
+            pltpu.VMEM((2,) + block, part.dtype),
+            pltpu.VMEM(block, part.dtype),
+            pltpu.VMEM(block, part.dtype),
+            pltpu.VMEM(block, part.dtype),
+        ]
+        + [pltpu.SemaphoreType.DMA((steps,))] * 8,
+        compiler_params=pltpu.CompilerParams(
+            collective_id=collective_id, has_side_effects=True, vmem_limit_bytes=40 << 20
+        ),
+    )(part)
 
 
 def contract_rows(left_side, right_side):
@@ -75,50 +340,50 @@
     resid_f = resid.astype(jnp.float32)
     inv_rms = lax.rsqrt(jnp.mean(resid_f * resid_f, axis=-1, keepdims=True) + 1e-06)
     normed = (resid_f * inv_rms * norm_gain).astype(jnp.bfloat16)
-    scaled = (route_weights[:, :, None] * grad_out.astype(jnp.float32)[:, None, :]).astype(
-        jnp.bfloat16
-    )
-    scaled = scaled.reshape(2 * tok_rows, model_width)
-    route_ids = routes.reshape(-1)
-    one_hot = (route_ids[:, None] == jnp.arange(sp_count, dtype=jnp.int32)[None, :]).astype(
-        jnp.int32
-    )
-    slot_rank = jnp.sum(jnp.cumsum(one_hot, axis=0) * one_hot, axis=1) - 1
-    slot_index = route_ids * capacity + slot_rank
-    slot_table = jnp.full((sp_count * capacity,), 2 * tok_rows, jnp.int32)
-    slot_table = slot_table.at[slot_index].set(jnp.arange(2 * tok_rows, dtype=jnp.int32))
-    normed_pad = jnp.concatenate([normed, jnp.zeros((1, model_width), jnp.bfloat16)], axis=0)
-    scaled_pad = jnp.concatenate([scaled, jnp.zeros((1, model_width), jnp.bfloat16)], axis=0)
+    my_sp = lax.axis_index("sp")
+    away = (routes - my_sp) % sp_count
+    steps_away = jnp.arange(sp_count, dtype=jnp.int32)
+    named = away[:, :, None] == steps_away[None, None, :]
+    chosen = jnp.any(named, axis=1)
+    weight_of = jnp.sum(jnp.where(named, route_weights[:, :, None], 0.0), axis=1)
+    token_ids = jnp.arange(tok_rows, dtype=jnp.int32)
+    earlier = (token_ids[None, :] < token_ids[:, None]).astype(jnp.bfloat16)
+    rank = jnp.dot(earlier, chosen.astype(jnp.bfloat16), preferred_element_type=jnp.float32)
+    rank = jnp.where(chosen, rank, -1.0).astype(jnp.int32)
+    slots = jnp.arange(capacity, dtype=jnp.int32)
+    held = rank.T[:, None, :] == slots[None, :, None]
+    slot_weight = jnp.sum(jnp.where(held, weight_of.T[:, None, :], 0.0), axis=2)
+    pick = held.astype(jnp.bfloat16).reshape(sp_count * capacity, tok_rows)
     first_col = lax.axis_index("tp") * col_count
-    normed_part = lax.dynamic_slice_in_dim(normed_pad, first_col, col_count, 1)
-    scaled_part = lax.dynamic_slice_in_dim(scaled_pad, first_col, col_count, 1)
-    send_rows = normed_part[slot_table // 2].reshape(sp_count, capacity, col_count)
-    send_cots = scaled_part[slot_table].reshape(sp_count, capacity, col_count)
-    part_rows, part_cots = (
-        lax.all_to_all(send_rows, "sp", split_axis=0, concat_axis=0, tiled=True),
-        lax.all_to_all(send_cots, "sp", split_axis=0, concat_axis=0, tiled=True),
-    )
-    routed_rows, routed_cots = (
-        lax.all_gather(part_rows, "tp", axis=2, tiled=True),
-        lax.all_gather(part_cots, "tp", axis=2, tiled=True),
+    normed_part = lax.dynamic_slice_in_dim(normed, first_col, col_count, 1)
+    cots_part = lax.dynamic_slice_in_dim(grad_out, first_col, col_count, 1)
+    send_rows = jnp.dot(pick, normed_part, preferred_element_type=jnp.float32).astype(jnp.bfloat16)
+    send_cots = jnp.dot(pick, cots_part, preferred_element_type=jnp.float32)
+    send_cots = (send_cots * slot_weight.reshape(-1, 1)).astype(jnp.bfloat16)
+    routed_rows, routed_cots = spread(
+        (
+            send_rows.reshape(sp_count, capacity, col_count),
+            send_cots.reshape(sp_count, capacity, col_count),
+        ),
+        True,
+        True,
+        False,
+        0,
     )
     routed_rows = routed_rows.reshape(sp_count * capacity, model_width)
     routed_cots = routed_cots.reshape(sp_count * capacity, model_width)
     gate_grad, up_grad, down_grad, partial_value = expert_backward(
         routed_rows, routed_cots, gate_weight[0], up_weight[0], down_weight[0]
     )
-    row_grad = lax.psum_scatter(
-        partial_value.reshape(sp_count, capacity, model_width).astype(jnp.bfloat16),
-        "tp",
-        scatter_dimension=2,
-        tiled=True,
-    )
-    returned = lax.all_to_all(row_grad, "sp", split_axis=0, concat_axis=0, tiled=True).reshape(
-        sp_count * capacity, col_count
-    )
-    normed_part_grad = returned[slot_index].reshape(tok_rows, 2, col_count).astype(jnp.float32)
-    normed_part_grad = normed_part_grad.sum(axis=1).astype(jnp.bfloat16)
-    normed_grad = lax.all_gather(normed_part_grad, "tp", axis=1, tiled=True)
+    returned = combine(
+        partial_value.reshape(sp_count, capacity, model_width).astype(jnp.bfloat16), 1
+    ).reshape(sp_count * capacity, col_count)
+    normed_part_grad = contract_rows(pick, returned).astype(jnp.bfloat16)
+    chunks = 4
+    (normed_grad,) = spread(
+        (normed_part_grad.reshape(chunks, tok_rows // chunks, col_count),), False, True, False, 2
+    )
+    normed_grad = normed_grad.reshape(tok_rows, model_width)
     feature_grad = normed_grad.astype(jnp.float32) * norm_gain
     cubed = inv_rms * inv_rms * inv_rms
     resid_grad = (
@@ -135,8 +400,17 @@
     pre_act = chan_normed * conv_gain
     sigma_conv = jax.nn.sigmoid(pre_act)
     conv_out = (pre_act * sigma_conv).astype(jnp.bfloat16)
-    proj_grad = lax.psum_scatter(
-        contract_rows(resid_grad, conv_out), "sp", scatter_dimension=0, tiled=True
+    all_out, reach = conv_out, 1
+    while reach < sp_count:
+        more = min(reach, sp_count - reach)
+        all_out = jnp.concatenate([all_out, rotated(all_out[: more * tok_rows], "sp", reach)])
+        reach += more
+    share = tok_rows // tp_count
+    tokens_part = lax.dynamic_slice_in_dim(resid_grad, lax.axis_index("tp") * share, share, 0)
+    by_feature = tokens_part.reshape(share, sp_count, model_width // sp_count).transpose(1, 0, 2)
+    (feature_cols,) = spread((by_feature,), True, False, True, 3)
+    proj_grad = contract_rows(
+        feature_cols.reshape(sp_count * tok_rows, model_width // sp_count), all_out
     )
     out_grad = jnp.dot(resid_grad, proj_weight, preferred_element_type=jnp.float32)
     normal_grad = (

time: 287 us -> 174 us (0.61)
  waiting for transfers between devices: 138 us -> 11.7 us
  Pallas kernels: 0 us -> 123 us
  blocking collectives: 51.2 us -> 0 us
  local copies, waits for them, and re-layouts: 28.1 us -> 2.1 us
  between operations: 14.2 us -> 1.11 us
  matrix products: 34.8 us -> 24.9 us
  other arithmetic: 12.3 us -> 6.96 us
  starting transfers between devices: 7.41 us -> 3.24 us
    pallas_call x0 -> x4, Pallas kernels: none -> 123 us  [the longest x3 85.8 us: spread(): pl.pallas_call(functools.partial(spread_kernel, count, steps, over_sp, in...]
    reduce_scatter x2 -> x0, waiting for transfers between devices: 88.9 us -> none  [the longest x1 51.1 us: local(): lax.psum_scatter(contract_rows(resid_grad, conv_out), 'sp', scatter_dimen...]
    all_to_all x2 -> x0, blocking collectives: 51.2 us -> none  [the longest x1 27.6 us: local(): lax.all_to_all(send_rows, 'sp', split_axis=0, concat_axis=0, tiled=True)]
    all_gather x3 -> x0, waiting for transfers between devices: 28.1 us -> none  [the longest x1 19.2 us: local(): lax.all_gather(part_cots, 'tp', axis=2, tiled=True)]
    all_to_all x1 -> x0, waiting for transfers between devices: 20 us -> none  [local(): lax.all_to_all(row_grad, 'sp', split_axis=0, concat_axis=0, tiled=True)]
    mul x5 -> x1, local copies, waits for them, and re-layouts: 11.9 us -> 0.07 us  [local(): send_cots = (send_cots * slot_weight.reshape(-1, 1)).astype(jnp.bfloat16)]
    ppermute x0 -> x3, waiting for transfers between devices: none -> 11.7 us  [rotated(): lax.ppermute(block, axis, [(i, (i + distance) % count) for i in range(cou...]
    gather x3 -> x0, local copies, waits for them, and re-layouts: 9.26 us -> none  [the longest x1 3.32 us: local(): send_cots = scaled_part[slot_table].reshape(sp_count, capacity, col_count)]
  transfers between devices with their start and end apart: 7 -> 4, of which waited for: 6 -> 1; matrix products, arithmetic and copies ran while one was open for 14% -> 7% of each run, Pallas kernels for 0% -> 14%
where the time goes in v1:
time: 174 us; the launch traced here: 173 us
  Pallas kernels  123 us (71%)
  matrix products  24.9 us (14%)
  waiting for transfers between devices  11.7 us (7%)
  other arithmetic  6.96 us (4%)
  starting transfers between devices  3.24 us (2%)
  local copies, waits for them, and re-layouts  2.1 us (1%)
    pallas_call x3, Pallas kernels, spread(): pl.pallas_call(functools.partial(spread_kernel, count, steps, over_sp, in...  85.8 us
    pallas_call x1, Pallas kernels, combine(): pl.pallas_call(functools.partial(combine_kernel, steps), out_shape=jax.Sh...  37.4 us
    ppermute x3, waiting for transfers between devices, rotated(): lax.ppermute(block, axis, [(i, (i + distance) % count) for i in range(cou...  11.7 us
    dot_general x5, matrix products, contract_rows(): lax.dot_general(left_side, right_side, (((0,), (0,)), ((), ())), preferre...  11.2 us
    dot_general x3, matrix products, contract_cols(): lax.dot_general(left_side, right_side, (((1,), (1,)), ((), ())), preferre...  6.13 us
  transfers between devices with their start and end apart: 4, of which 1 were waited for; matrix products, arithmetic and copies ran while one was open for 7% of the time, Pallas kernels for 14%

profile of v1, /device:TPU:0, one launch (start us, length us, event | category | flops | bytes accessed | tf_op | source)
XLA Modules:
  0.0 173.2 jit_solution(16583490007494753411)
XLA Ops:
  0.6 0.0 copy-start
  0.7 0.0 copy-start.1
  0.7 0.0 copy-start.9
  0.7 0.0 copy-start.10
  0.7 0.0 copy-start.7
  0.7 3.0 %convert_element_type.76 = f32[256,2048]{1,0:T(8,128)} convert(bf16[256,2048]{1,0:T(8,128)(2,1)} %param.15) | non-fusion elementwise | flops 524288 | bytes 3145728 | tf_op jit(solution)/shard_map/convert_element_type | solution.py:340
  3.7 0.0 copy-done.1
  3.7 0.3 multiply_reduce_fusion
  4.0 0.1 eq.45
  4.0 0.0 copy-done.9
  4.1 0.2 fusion.21
  4.3 0.0 copy-done.10
  4.3 0.2 bitcast_compare_fusion
  4.5 0.2 select_reduce_fusion
  4.7 0.1 mul.184
  4.8 0.0 copy-done.7
  4.8 0.1 dynamic-slice
  4.8 1.3 multiply_convert_fusion
  6.2 0.0 copy-start.4
  6.2 1.6 convolution_convert_fusion.3
  7.8 51.9 %shard_map.181 = (bf16[8,96,2048]{2,1,0:T(8,128)(2,1)S(1)}, bf16[8,96,2048]{2,1,0:T(8,128)(2,1)S(1)}) custom-call(bf16[8,96,512]{2,1,0:T(8,128)(2,1)S(1)} %bitcast.80, bf16[8,96,512]{2,1,0:T(8,128)(2,1)S(1)} %bitcast.79), custom_call_target="tpu_custom_call" | custom-call | tf_op jit(solution)/shard_map/pallas_call | solution.py:152
  59.7 0.0 copy-done.4
  59.7 1.8 %fusion.10 = f32[768,384]{1,0:T(8,128)S(1)} fusion(bf16[768,2048]{1,0:T(8,128)(2,1)S(1)} %bitcast.84, bf16[1,2048,384]{2,1,0:T(8,128)(2,1)S(1)} %copy-done.4), kind=kOutput, calls=%fused_computation.16 | convolution fusion | flops 1207959552 | bytes 5898240 | tf_op jit(solution)/shard_map/dot_general | solution.py:299
  61.5 0.0 copy-start.12
  61.5 1.8 %fusion.16 = f32[768,384]{1,0:T(8,128)S(1)} fusion(bf16[768,2048]{1,0:T(8,128)(2,1)S(1)} %bitcast.85, bf16[1,2048,384]{2,1,0:T(8,128)(2,1)S(1)} %copy-done), kind=kOutput, calls=%fused_computation.22 | convolution fusion | flops 1207959552 | bytes 5898240 | tf_op jit(solution)/shard_map/dot_general | solution.py:298
  63.3 2.5 %select_convert_fusion = (bf16[768,384]{1,0:T(8,128)(2,1)S(1)}, bf16[768,384]{1,0:T(8,128)(2,1)S(1)}) fusion(f32[768,384]{1,0:T(8,128)S(1)} %fusion.10, f32[768,384]{1,0:T(8,128)S(1)} %fusion.16, bf16[768,2048]{1,0:T(8,128)(2,1)S(1)} %bitcast.88, bf16[1,384,2048]{2,1,0:T(8,128)(2,1)S(1)} %copy-done.12), kind=kOutput, calls=%fused_computation.29 | convolution fusion | flops 1214742528 | bytes 8257536 | tf_op jit(solution)/shard_map/dot_general | solution.py:292
  65.8 1.8 %fusion.14 = f32[768,2048]{1,0:T(8,128)S(1)} fusion(bf16[768,384]{1,0:T(8,128)(2,1)S(1)} %get-tuple-element.13, bf16[1,2048,384]{2,1,0:T(8,128)(2,1)S(1)} %copy-done), kind=kOutput, calls=%fused_computation.20 | convolution fusion | flops 1207959552 | bytes 8454144 | tf_op jit(solution)/shard_map/dot_general | solution.py:292
  67.6 1.9 %add_convert_fusion = bf16[768,2048]{1,0:T(8,128)(2,1)S(1)} fusion(f32[768,2048]{1,0:T(8,128)S(1)} %fusion.14, bf16[768,384]{1,0:T(8,128)(2,1)S(1)} %get-tuple-element.12, bf16[1,2048,384]{2,1,0:T(8,128)(2,1)S(1)} %copy-done.4), kind=kOutput, calls=%fused_computation | convolution fusion | flops 1211105280 | bytes 11599872 | tf_op jit(solution)/shard_map/dot_general | solution.py:292
  69.5 37.4 %shard_map.182 = bf16[8,96,512]{2,1,0:T(8,128)(2,1)S(1)} custom-call(bf16[8,96,2048]{2,1,0:T(8,128)(2,1)S(1)} %bitcast.78), custom_call_target="tpu_custom_call" | custom-call | tf_op jit(solution)/shard_map/pallas_call | solution.py:267
  106.9 0.4 fusion.18
  107.3 0.0 copy-start.5
  107.3 0.0 copy-start.3
  107.4 9.8 %shard_map.183 = bf16[4,64,2048]{2,1,0:T(8,128)(2,1)S(1)} custom-call(bf16[4,64,512]{2,1,0:T(8,128)(2,1)S(1)} %bitcast.83), custom_call_target="tpu_custom_call" | custom-call | tf_op jit(solution)/shard_map/pallas_call | solution.py:152
  117.2 0.4 fusion.8
  117.6 0.1 convert_reduce_fusion
  117.7 0.2 fusion.62
  117.9 0.0 copy-start.11
  118.0 0.0 copy-start.13
  118.0 0.7 fusion.7
  118.7 0.0 copy-done.11
  118.7 0.3 copy-done.13
  119.0 0.6 fusion.75
  119.6 0.2 fusion.61
  119.8 0.2 collective-permute-start
  120.0 1.3 collective-permute-start.3
  121.3 3.0 %fusion = bf16[1,2048,384]{2,1,0:T(8,128)(2,1)} fusion(bf16[768,2048]{1,0:T(8,128)(2,1)S(1)} %bitcast.86, bf16[768,384]{1,0:T(8,128)(2,1)S(1)} %get-tuple-element.13), kind=kOutput, calls=%fused_computation.4 | convolution fusion | flops 1208745984 | bytes 5308416 | tf_op jit(solution)/shard_map/dot_general | solution.py:286
  124.3 0.0 copy-done.2
  124.3 2.7 %fusion.2 = bf16[1,384,2048]{2,1,0:T(8,128)(2,1)} fusion(bf16[768,2048]{1,0:T(8,128)(2,1)S(1)} %bitcast.89, f32[768,384]{1,0:T(8,128)S(1)} %fusion.10, f32[768,384]{1,0:T(8,128)S(1)} %fusion.16), kind=kOutput, calls=%fused_computation.6 | convolution fusion | flops 1211695104 | bytes 7077888 | tf_op jit(solution)/shard_map/dot_general | solution.py:286
  127.0 3.0 %fusion.1 = bf16[1,2048,384]{2,1,0:T(8,128)(2,1)} fusion(bf16[768,2048]{1,0:T(8,128)(2,1)S(1)} %bitcast.87, bf16[768,384]{1,0:T(8,128)(2,1)S(1)} %get-tuple-element.12), kind=kOutput, calls=%fused_computation.5 | convolution fusion | flops 1208745984 | bytes 5308416 | tf_op jit(solution)/shard_map/dot_general | solution.py:286
  130.0 0.0 collective-permute-done
  130.1 1.6 collective-permute-start.1
  131.7 1.0 constant_dynamic-slice_fusion
  132.7 0.0 copy-start.14
  132.7 24.1 %shard_map.184 = bf16[8,4,64,256]{3,2,1,0:T(8,128)(2,1)S(1)} custom-call(bf16[8,64,256]{2,1,0:T(8,128)(2,1)S(1)} %bitcast.82), custom_call_target="tpu_custom_call" | custom-call | tf_op jit(solution)/shard_map/pallas_call | solution.py:152
  156.9 0.0 collective-permute-done.3
  157.0 0.0 collective-permute-done.1
  157.0 0.1 collective-permute-start.2
  157.1 0.0 copy-done.14
  157.1 0.0 copy-start.6
  157.1 0.4 convolution_select_fusion
  157.5 0.4 copy-done.6
  157.9 1.6 multiply_convert_fusion.3
  159.5 11.7 %collective-permute-done.2 = bf16[1024,128]{1,0:T(8,128)(2,1)} collective-permute-done((bf16[1024,128]{1,0:T(8,128)(2,1)S(1)}, bf16[1024,128]{1,0:T(8,128)(2,1)}, u32[]{:S(2)}, u32[]{:S(2)}) %collective-permute-start.2) | collective-permute-done | bytes 262176 | tf_op jit(solution)/shard_map/ppermute | solution.py:27
  171.2 2.1 %fusion.27 = f32[256,128]{1,0:T(8,128)} fusion(bf16[2048,256]{1,0:T(8,128)(2,1)S(1)} %bitcast.81, bf16[1024,128]{1,0:T(8,128)(2,1)} %collective-permute-done.2, bf16[512,128]{1,0:T(8,128)(2,1)S(1)} %collective-permute-done.1, bf16[256,128]{1,0:T(8,128)(2,1)S(1)} %collective-permute-done, bf16[256,128]{1,0:T(8,128)(2,1)S(1)} %get-tuple-element.17), kind=kOutput, calls=%fused_computation.49 | convolution fusion | flops 136314880 | bytes 1703936 | tf_op jit(solution)/shard_map/dot_general | solution.py:286
  (27 shorter events, 0.2 us)
Async XLA Ops:
  0.6 60.9 %copy-start = (bf16[1,2048,384]{2,1,0:T(8,128)(2,1)S(1)}, bf16[1,2048,384]{2,1,0:T(8,128)(2,1)}, u32[]{:S(2)}) copy-start(bf16[1,2048,384]{2,1,0:T(8,128)(2,1)} %param.19) | copy-start | bytes 4718596
  0.7 3.0 %copy-start.1 = (bf16[256,2048]{1,0:T(8,128)(2,1)S(1)}, bf16[256,2048]{1,0:T(8,128)(2,1)}, u32[]{:S(2)}) copy-start(bf16[256,2048]{1,0:T(8,128)(2,1)} %param.15) | copy-start | bytes 3145732
  0.7 3.4 %copy-start.9 = (s32[256,2]{0,1:T(2,128)S(1)}, s32[256,2]{0,1:T(2,128)}, u32[]{:S(2)}) copy-start(s32[256,2]{0,1:T(2,128)} %param.17) | copy-start | bytes 6148
  0.7 3.6 %copy-start.10 = (f32[256,2]{0,1:T(2,128)S(1)}, f32[256,2]{0,1:T(2,128)}, u32[]{:S(2)}) copy-start(f32[256,2]{0,1:T(2,128)} %param.18) | copy-start | bytes 6148
  0.7 4.1 %copy-start.7 = (f32[2048]{0:T(1024)S(1)}, f32[2048]{0:T(1024)}, u32[]{:S(2)}) copy-start(f32[2048]{0:T(1024)} %param.16) | copy-start | bytes 24580
  6.2 53.5 %copy-start.4 = (bf16[1,2048,384]{2,1,0:T(8,128)(2,1)S(1)}, bf16[1,2048,384]{2,1,0:T(8,128)(2,1)}, u32[]{:S(2)}) copy-start(bf16[1,2048,384]{2,1,0:T(8,128)(2,1)} %param.20) | copy-start | bytes 4718596
  61.5 1.8 %copy-start.12 = (bf16[1,384,2048]{2,1,0:T(8,128)(2,1)S(1)}, bf16[1,384,2048]{2,1,0:T(8,128)(2,1)}, u32[]{:S(2)}) copy-start(bf16[1,384,2048]{2,1,0:T(8,128)(2,1)} %param.21) | copy-start | bytes 4718596
  107.3 10.3 %copy-start.5 = (bf16[256,128]{1,0:T(8,128)(2,1)S(1)}, bf16[256,128]{1,0:T(8,128)(2,1)}, u32[]{:S(2)}) copy-start(bf16[256,128]{1,0:T(8,128)(2,1)} %param.23) | copy-start | bytes 196612
  107.3 10.6 %copy-start.3 = (bf16[256,2048]{1,0:T(8,128)(2,1)S(1)}, bf16[256,2048]{1,0:T(8,128)(2,1)}, u32[]{:S(2)}) copy-start(bf16[256,2048]{1,0:T(8,128)(2,1)} %param.14) | copy-start | bytes 3145732
  117.9 0.8 copy-start.11
  118.0 1.0 copy-start.13
  119.0 5.3 %copy-start.2 = (bf16[256,2048]{1,0:T(8,128)(2,1)}, bf16[256,2048]{1,0:T(8,128)(2,1)S(1)}, u32[]{:S(2)}) copy-start(bf16[256,2048]{1,0:T(8,128)(2,1)S(1)} %fusion.7) | copy-start | bytes 3145732
  119.8 10.3 %collective-permute-start = (bf16[256,128]{1,0:T(8,128)(2,1)S(1)}, bf16[256,128]{1,0:T(8,128)(2,1)S(1)}, u32[]{:S(2)}, u32[]{:S(2)}) collective-permute-start(bf16[256,128]{1,0:T(8,128)(2,1)S(1)} %get-tuple-element.17), channel_id=1, source_target_pairs={{0,4},{4,8},{8,12},{12,16},{16,20},{20,24},{24,28},{28,0},{1,5},{5... | collective-permute-start | bytes 196616 | tf_op jit(solution)/shard_map/ppermute | solution.py:27
  120.0 36.8 %collective-permute-start.3 = (f32[30,128]{1,0:T(8,128)S(1)}, f32[30,128]{1,0:T(8,128)S(1)}, u32[]{:S(2)}, u32[]{:S(2)}) collective-permute-start(f32[30,128]{1,0:T(8,128)S(1)} %slice.8), channel_id=1, source_target_pairs={{4,0},{8,4},{12,8},{16,12},{20,16},{24,20},{28,24},{5,1},{9,5},{13... | collective-permute-start | bytes 46088 | tf_op jit(solution)/shard_map/ppermute | solution.py:22
  130.0 26.8 %copy-start.8 = (f32[31,128]{1,0:T(8,128)S(1)}, f32[31,128]{1,0:T(8,128)}, u32[]{:S(2)}) copy-start(f32[31,128]{1,0:T(8,128)} %param.25) | copy-start | bytes 47620
  130.1 26.9 %collective-permute-start.1 = (bf16[512,128]{1,0:T(8,128)(2,1)S(1)}, bf16[512,128]{1,0:T(8,128)(2,1)S(1)}, u32[]{:S(2)}, u32[]{:S(2)}) collective-permute-start(bf16[512,128]{1,0:T(8,128)(2,1)S(1)} %pad_maximum_fusion.1), channel_id=1, source_target_pairs={{0,8},{4,12},{8,16},{12,20},{16,24},{20,28},{24,0},{28,4},{1,9},{5... | collective-permute-start | bytes 393224 | tf_op jit(solution)/shard_map/ppermute | solution.py:27
  132.7 24.4 %copy-start.14 = (pred[8,36]{0,1:T(8,128)(4,1)S(1)}, pred[8,36]{0,1:T(8,128)(4,1)}, u32[]{:S(2)}) copy-start(pred[8,36]{0,1:T(8,128)(4,1)} %constant.73) | copy-start | bytes 868
  157.0 14.2 %collective-permute-start.2 = (bf16[1024,128]{1,0:T(8,128)(2,1)S(1)}, bf16[1024,128]{1,0:T(8,128)(2,1)}, u32[]{:S(2)}, u32[]{:S(2)}) collective-permute-start(bf16[1024,128]{1,0:T(8,128)(2,1)S(1)} %pad_maximum_fusion), channel_id=1, source_target_pairs={{0,16},{4,20},{8,24},{12,28},{16,0},{20,4},{24,8},{28,12},{1,17},{... | collective-permute-start | bytes 786440 | tf_op jit(solution)/shard_map/ppermute | solution.py:27
  157.1 0.8 copy-start.6

commit v2 on v1

--- a/solution.py
+++ b/solution.py
@@ -20,11 +20,6 @@
     devices = range(lax.axis_size(axis))
     route = [(i - distance, i) for i in devices if i - distance in devices]
     return lax.ppermute(block, axis, route)
-
-
-def rotated(block, axis, distance):
-    count = lax.axis_size(axis)
-    return lax.ppermute(block, axis, [(i, (i + distance) % count) for i in range(count)])
 
 
 def tp_places():
@@ -54,9 +49,26 @@
     pl.semaphore_wait(barrier, total)
 
 
-def spread_kernel(count, steps, over_sp, in_lanes, absolute, *refs):
-    sends, outs = refs[:count], refs[count : 2 * count]
-    own_sem, a_send, a_recv, b_send, f_send, c_send, near_recv, fwd_recv, far_recv = refs[2 * count :]
+def crossing_first(steps, k):
+    return steps // 2 + ((k + 1) // 2) * (2 * (k % 2) - 1)
+
+
+def looped(first, last, body):
+    def step(k, carry):
+        body(k)
+        return carry
+
+    lax.fori_loop(first, last, step, 0)
+
+
+def spread_kernel(count, steps, over_sp, in_lanes, absolute, beside, sp_count, *refs):
+    refs = list(refs)
+    sends, refs = refs[:count], refs[count:]
+    fulls, refs = (refs[:count], refs[count:]) if over_sp else (None, refs)
+    side, refs = (refs[0], refs[1:]) if beside else (None, refs)
+    outs, refs = refs[:count], refs[count:]
+    side_out, refs = (refs[0], refs[1:]) if beside else (None, refs)
+    own_sem, a_send, a_recv, b_send, f_send, c_send, near_recv, fwd_recv, far_recv = refs[:9]
     s = lax.axis_index("sp")
     t, near, far, _ = tp_places()
     width = sends[0].shape[-1]
@@ -70,6 +82,8 @@
         return sends[c].at[(s + d) % steps if absolute else d]
 
     def own(c, d):
+        if over_sp:
+            return pltpu.make_async_copy(fulls[c], outs[c].at[0], own_sem.at[c, 0])
         return pltpu.make_async_copy(source(c, d), place(c, d, t), own_sem.at[c, d])
 
     def to_sp(c, d):
@@ -101,18 +115,19 @@
     def fwd_copy(c, d):
         return to_tp(c, d, far, near, c_send, fwd_recv)
 
-    def loop(first, last, body):
-        def step(d, carry):
-            for c in range(count):
-                body(c, d)
-            return carry
-
-        lax.fori_loop(first, last, step, 0)
-
-    meet(steps, over_sp, near, far)
-    remote_from = 1 if over_sp else steps
-    loop(0, remote_from, lambda c, d: own(c, d).start())
-    loop(remote_from, steps, lambda c, d: to_sp(c, d).start())
+    def side_copy(d):
+        side_send, side_recv = refs[10:12]
+        return pltpu.make_async_remote_copy(
+            src_ref=side,
+            dst_ref=side_out.at[d],
+            send_sem=side_send.at[d],
+            recv_sem=side_recv.at[d],
+            device_id=((s + d) % sp_count, t),
+            device_id_type=MESH,
+        )
+
+    def own_side():
+        return pltpu.make_async_copy(side, side_out.at[0], refs[9].at[0])
 
     def share(c, d):
         far_copy(c, d).start()
@@ -121,44 +136,86 @@
     def forward(c, d):
         far_copy(c, d).wait_recv()
         fwd_copy(c, d).start()
-
-    def share_own(c, d):
-        own(c, d).wait()
-        share(c, d)
-
-    def share_arrived(c, d):
-        to_sp(c, d).wait_recv()
-        share(c, d)
-        forward(c, d - 1)
-
-    loop(0, remote_from, share_own)
-    loop(remote_from, steps, share_arrived)
-    loop(steps - 1 if over_sp else 0, steps, forward)
 
     def finish(c, d):
         near_copy(c, d).wait()
         far_copy(c, d).wait_send()
         fwd_copy(c, d).wait()
 
-    loop(0, steps, finish)
-    loop(remote_from, steps, lambda c, d: to_sp(c, d).wait_send())
-
-
-def spread(sends, over_sp, in_lanes, absolute, collective_id):
+    def loop(first, last, body):
+        def each(k):
+            d = crossing_first(steps, k) if over_sp else k
+            for c in range(count):
+                body(c, d)
+
+        looped(first, last, each)
+
+    meet(sp_count, over_sp or beside, near, far)
+    if over_sp:
+        loop(0, steps - 1, lambda c, d: to_sp(c, d).start())
+        for c in range(count):
+            own(c, 0).start()
+
+        def pass_on(k):
+            for c in range(count):
+                d = crossing_first(steps, k)
+                to_sp(c, d).wait_recv()
+                share(c, d)
+
+        def pass_on_twice(k):
+            pass_on(k)
+            for c in range(count):
+                forward(c, crossing_first(steps, k - 1))
+
+        pass_on(0)
+        looped(1, steps - 1, pass_on_twice)
+        loop(steps - 2, steps - 1, forward)
+        loop(0, steps - 1, finish)
+        loop(0, steps - 1, lambda c, d: to_sp(c, d).wait_send())
+        for c in range(count):
+            own(c, 0).wait()
+    else:
+        loop(0, steps, lambda c, d: own(c, d).start())
+        if beside:
+            looped(0, sp_count - 1, lambda k: side_copy(crossing_first(sp_count, k)).start())
+            own_side().start()
+
+        def share_own(c, d):
+            own(c, d).wait()
+            share(c, d)
+
+        loop(0, steps, share_own)
+        loop(0, steps, forward)
+        loop(0, steps, finish)
+        if beside:
+            looped(0, sp_count - 1, lambda k: side_copy(crossing_first(sp_count, k)).wait())
+            own_side().wait()
+
+
+def spread(sends, fulls, side, in_lanes, absolute, collective_id):
     count = len(sends)
     steps, rows, width = sends[0].shape
-    tp_count = lax.axis_size("tp")
+    tp_count, sp_count = lax.axis_size("tp"), lax.axis_size("sp")
+    over_sp, beside = fulls is not None, side is not None
     shape = (steps, rows, tp_count * width) if in_lanes else (steps, tp_count, rows, width)
+    out_shape = [jax.ShapeDtypeStruct(shape, x.dtype) for x in sends]
+    operands = list(sends) + (list(fulls) if over_sp else []) + ([side] if beside else [])
+    scratch = [pltpu.SemaphoreType.DMA((count, steps))] * 9
+    if beside:
+        out_shape.append(jax.ShapeDtypeStruct((sp_count,) + side.shape, side.dtype))
+        scratch += [pltpu.SemaphoreType.DMA((1,))] + [pltpu.SemaphoreType.DMA((sp_count,))] * 2
     return pl.pallas_call(
-        functools.partial(spread_kernel, count, steps, over_sp, in_lanes, absolute),
-        out_shape=tuple(jax.ShapeDtypeStruct(shape, x.dtype) for x in sends),
-        in_specs=[pl.BlockSpec(memory_space=pltpu.VMEM)] * count,
-        out_specs=tuple(pl.BlockSpec(memory_space=pltpu.VMEM) for _ in sends),
-        scratch_shapes=[pltpu.SemaphoreType.DMA((count, steps))] * 9,
+        functools.partial(
+            spread_kernel, count, steps, over_sp, in_lanes, absolute, beside, sp_count
+        ),
+        out_shape=tuple(out_shape),
+        in_specs=[pl.BlockSpec(memory_space=pltpu.VMEM)] * len(operands),
+        out_specs=tuple(pl.BlockSpec(memory_space=pltpu.VMEM) for _ in out_shape),
+        scratch_shapes=scratch,
         compiler_params=pltpu.CompilerParams(
             collective_id=collective_id, has_side_effects=True, vmem_limit_bytes=40 << 20
         ),
-    )(*sends)
+    )(*operands)
 
 
 def combine_kernel(
@@ -208,13 +265,6 @@
             device_id_type=MESH,
         )
 
-    def loop(first, last, body):
-        def step(d, carry):
-            body(d)
-            return carry
-
-        lax.fori_loop(first, last, step, 0)
-
     meet(steps, True, near, far)
 
     def open_up(d):
@@ -238,17 +288,21 @@
         total[d] = whole(d)
         back(d).start()
 
-    loop(1, steps, open_up)
+    def at(k):
+        return crossing_first(steps, k)
+
+    lag = min(3, steps - 1)
+    looped(0, steps - 1, lambda k: open_up(at(k)))
     open_up(0)
-    add_pair(1)
-
-    def middle(d):
-        add_pair(d)
-        send_back(d - 1)
-
-    loop(2, steps, middle)
+    looped(0, lag, lambda k: add_pair(at(k)))
+
+    def middle(k):
+        add_pair(at(k))
+        send_back(at(k - lag))
+
+    looped(lag, steps - 1, middle)
     add_pair(0)
-    send_back(steps - 1)
+    looped(steps - 1 - lag, steps - 1, lambda k: send_back(at(k)))
     out[0] = whole(0)
 
     def finish(d):
@@ -256,8 +310,8 @@
         for_diag(d).wait_send()
         far_copy(d).wait_send()
 
-    loop(0, steps, finish)
-    loop(1, steps, lambda d: back(d).wait())
+    looped(0, steps, finish)
+    looped(1, steps, lambda d: back(d).wait())
 
 
 def combine(part, collective_id):
@@ -357,15 +411,21 @@
     first_col = lax.axis_index("tp") * col_count
     normed_part = lax.dynamic_slice_in_dim(normed, first_col, col_count, 1)
     cots_part = lax.dynamic_slice_in_dim(grad_out, first_col, col_count, 1)
+    slot_weight = slot_weight.reshape(-1, 1)
     send_rows = jnp.dot(pick, normed_part, preferred_element_type=jnp.float32).astype(jnp.bfloat16)
     send_cots = jnp.dot(pick, cots_part, preferred_element_type=jnp.float32)
-    send_cots = (send_cots * slot_weight.reshape(-1, 1)).astype(jnp.bfloat16)
+    send_cots = (send_cots * slot_weight).astype(jnp.bfloat16)
+    own_pick = pick[:capacity]
+    own_rows = jnp.dot(own_pick, normed, preferred_element_type=jnp.float32).astype(jnp.bfloat16)
+    own_cots = jnp.dot(own_pick, grad_out, preferred_element_type=jnp.float32)
+    own_cots = (own_cots * slot_weight[:capacity]).astype(jnp.bfloat16)
     routed_rows, routed_cots = spread(
         (
             send_rows.reshape(sp_count, capacity, col_count),
             send_cots.reshape(sp_count, capacity, col_count),
         ),
-        True,
+        (own_rows, own_cots),
+        None,
         True,
         False,
         0,
@@ -379,18 +439,6 @@
         partial_value.reshape(sp_count, capacity, model_width).astype(jnp.bfloat16), 1
     ).reshape(sp_count * capacity, col_count)
     normed_part_grad = contract_rows(pick, returned).astype(jnp.bfloat16)
-    chunks = 4
-    (normed_grad,) = spread(
-        (normed_part_grad.reshape(chunks, tok_rows // chunks, col_count),), False, True, False, 2
-    )
-    normed_grad = normed_grad.reshape(tok_rows, model_width)
-    feature_grad = normed_grad.astype(jnp.float32) * norm_gain
-    cubed = inv_rms * inv_rms * inv_rms
-    resid_grad = (
-        grad_out.astype(jnp.float32)
-        + inv_rms * feature_grad
-        - resid_f * cubed * jnp.mean(resid_f * feature_grad, axis=-1, keepdims=True)
-    ).astype(jnp.bfloat16)
     channels = conv_sum.shape[1]
     summed = conv_sum.astype(jnp.float32).reshape(tok_rows, channels // GROUP, GROUP)
     centre = summed - jnp.mean(summed, axis=-1, keepdims=True)
@@ -400,17 +448,34 @@
     pre_act = chan_normed * conv_gain
     sigma_conv = jax.nn.sigmoid(pre_act)
     conv_out = (pre_act * sigma_conv).astype(jnp.bfloat16)
-    all_out, reach = conv_out, 1
-    while reach < sp_count:
-        more = min(reach, sp_count - reach)
-        all_out = jnp.concatenate([all_out, rotated(all_out[: more * tok_rows], "sp", reach)])
-        reach += more
+    chunks = 4
+    normed_grad, all_out = spread(
+        (normed_part_grad.reshape(chunks, tok_rows // chunks, col_count),),
+        None,
+        conv_out,
+        True,
+        False,
+        2,
+    )
+    normed_grad = normed_grad.reshape(tok_rows, model_width)
+    feature_grad = normed_grad.astype(jnp.float32) * norm_gain
+    cubed = inv_rms * inv_rms * inv_rms
+    resid_grad = (
+        grad_out.astype(jnp.float32)
+        + inv_rms * feature_grad
+        - resid_f * cubed * jnp.mean(resid_f * feature_grad, axis=-1, keepdims=True)
+    ).astype(jnp.bfloat16)
     share = tok_rows // tp_count
+    feat_rows = model_width // sp_count
     tokens_part = lax.dynamic_slice_in_dim(resid_grad, lax.axis_index("tp") * share, share, 0)
-    by_feature = tokens_part.reshape(share, sp_count, model_width // sp_count).transpose(1, 0, 2)
-    (feature_cols,) = spread((by_feature,), True, False, True, 3)
+    by_feature = tokens_part.reshape(share, sp_count, feat_rows).transpose(1, 0, 2)
+    own_features = lax.dynamic_slice_in_dim(resid_grad, my_sp * feat_rows, feat_rows, 1)
+    (feature_cols,) = spread(
+        (by_feature,), (own_features.reshape(tp_count, share, feat_rows),), None, False, True, 3
+    )
     proj_grad = contract_rows(
-        feature_cols.reshape(sp_count * tok_rows, model_width // sp_count), all_out
+        feature_cols.reshape(sp_count * tok_rows, feat_rows),
+        all_out.reshape(sp_count * tok_rows, channels),
     )
     out_grad = jnp.dot(resid_grad, proj_weight, preferred_element_type=jnp.float32)
     normal_grad = (

time: 174 us -> 164 us (0.943)
  waiting for transfers between devices: 11.7 us -> 0.01 us
  Pallas kernels: 123 us -> 126 us
    pallas_call x3, Pallas kernels: 85.8 us -> 99.3 us  [spread(): pl.pallas_call(functools.partial(spread_kernel, count, steps, over_sp, in...]
    ppermute x3 -> x0, waiting for transfers between devices: 11.7 us -> none  [rotated(): lax.ppermute(block, axis, [(i, (i + distance) % count) for i in range(cou...]
    pallas_call x1, Pallas kernels: 37.4 us -> 26.4 us  [combine(): pl.pallas_call(functools.partial(combine_kernel, steps), out_shape=jax.Sh...]
    ppermute x3 -> x0, starting transfers between devices: 1.95 us -> none  [rotated(): lax.ppermute(block, axis, [(i, (i + distance) % count) for i in range(cou...]
    dot_general x0 -> x2, matrix products: none -> 1.94 us  [the longest x1 1.62 us: local(): jnp.dot(own_pick, normed, preferred_element_type=jnp.float32)]
  transfers between devices with their start and end apart: 4 -> 1, of which waited for: 1 -> 0; matrix products, arithmetic and copies ran while one was open for 7% -> 7% of each run, Pallas kernels for 14% -> 14%
where the time goes in v2:
time: 164 us
  Pallas kernels  126 us (77%)
  matrix products  24.6 us (15%)
  other arithmetic  7.44 us (5%)
  local copies, waits for them, and re-layouts  3.38 us (2%)
    pallas_call x3, Pallas kernels, spread(): pl.pallas_call(functools.partial(spread_kernel, count, steps, over_sp, in...  99.3 us
    pallas_call x1, Pallas kernels, combine(): pl.pallas_call(functools.partial(combine_kernel, steps), out_shape=jax.Sh...  26.4 us
    dot_general x5, matrix products, contract_rows(): lax.dot_general(left_side, right_side, (((0,), (0,)), ((), ())), preferre...  10.2 us
    dot_general x3, matrix products, contract_cols(): lax.dot_general(left_side, right_side, (((1,), (1,)), ((), ())), preferre...  6.13 us
  transfers between devices with their start and end apart: 1, of which 0 were waited for; matrix products, arithmetic and copies ran while one was open for 7% of the time, Pallas kernels for 14%

profile of v2, /device:TPU:0, one launch (start us, length us, event | category | flops | bytes accessed | tf_op | source)
XLA Modules:
  0.0 163.7 jit_solution(8322608788408878442)
XLA Ops:
  0.6 0.0 copy-start
  0.6 0.0 copy-start.1
  0.7 0.0 copy-start.6
  0.7 0.8 and_select_fusion
  1.5 0.2 fusion.25
  1.7 0.7 select_reduce_fusion.1
  2.4 0.1 iota_compare_fusion
  2.5 0.2 select_reduce_fusion
  2.7 0.1 mul.197
  2.8 0.1 eq.45
  2.9 0.2 bitcast_compare_fusion
  3.1 1.5 fusion.4
  4.6 0.0 copy-done.1
  4.6 0.0 copy-done.6
  4.6 1.3 fusion.6
  5.9 1.6 convolution_convert_fusion.3.refs_2_
  7.5 1.3 convolution_convert_fusion.4
  8.9 0.0 copy-done.2
  8.9 0.4 multiply_convert_fusion
  9.3 0.0 copy-start.4
  9.3 0.3 fusion.3.refs_3_
  9.6 60.3 %shard_map.181 = (bf16[8,96,2048]{2,1,0:T(8,128)(2,1)S(1)}, bf16[8,96,2048]{2,1,0:T(8,128)(2,1)S(1)}) custom-call(bf16[8,96,512]{2,1,0:T(8,128)(2,1)S(1)} %bitcast.91, bf16[8,96,512]{2,1,0:T(8,128)(2,1)S(1)} %bitcast.92, bf16[96,2048]{1,0:T(8,128)(2,1)S(1)} %convolution_convert_fusion.3.refs_2_, bf16[96,2048]{1,0:T(8,128)(2,1)S(1)} %fusion.3.refs_3_), custom_call_target="tpu_custom_call" | custom-call | tf_op jit(solution)/shard_map/pallas_call | solution.py:207
  69.9 0.0 copy-done.4
  69.9 1.8 %fusion.14 = f32[768,384]{1,0:T(8,128)S(1)} fusion(bf16[768,2048]{1,0:T(8,128)(2,1)S(1)} %bitcast.99, bf16[1,2048,384]{2,1,0:T(8,128)(2,1)S(1)} %copy-done.4), kind=kOutput, calls=%fused_computation.25 | convolution fusion | flops 1207959552 | bytes 5898240 | tf_op jit(solution)/shard_map/dot_general | solution.py:353
  71.7 0.0 copy-done
  71.7 0.0 copy-start.11
  71.7 1.8 %fusion.20 = f32[768,384]{1,0:T(8,128)S(1)} fusion(bf16[768,2048]{1,0:T(8,128)(2,1)S(1)} %bitcast.100, bf16[1,2048,384]{2,1,0:T(8,128)(2,1)S(1)} %copy-done), kind=kOutput, calls=%fused_computation.31 | convolution fusion | flops 1207959552 | bytes 5898240 | tf_op jit(solution)/shard_map/dot_general | solution.py:352
  73.5 0.0 copy-done.11
  73.5 2.5 %select_convert_fusion = (bf16[768,384]{1,0:T(8,128)(2,1)S(1)}, bf16[768,384]{1,0:T(8,128)(2,1)S(1)}) fusion(f32[768,384]{1,0:T(8,128)S(1)} %fusion.14, f32[768,384]{1,0:T(8,128)S(1)} %fusion.20, bf16[768,2048]{1,0:T(8,128)(2,1)S(1)} %bitcast.97, bf16[1,384,2048]{2,1,0:T(8,128)(2,1)S(1)} %copy-done.11), kind=kOutput, calls=%fused_computation.38 | convolution fusion | flops 1214742528 | bytes 8257536 | tf_op jit(solution)/shard_map/dot_general | solution.py:346
  76.0 1.8 %fusion.18 = f32[768,2048]{1,0:T(8,128)S(1)} fusion(bf16[768,384]{1,0:T(8,128)(2,1)S(1)} %get-tuple-element.17, bf16[1,2048,384]{2,1,0:T(8,128)(2,1)S(1)} %copy-done), kind=kOutput, calls=%fused_computation.29 | convolution fusion | flops 1207959552 | bytes 8454144 | tf_op jit(solution)/shard_map/dot_general | solution.py:346
  77.8 1.9 %add_convert_fusion = bf16[768,2048]{1,0:T(8,128)(2,1)S(1)} fusion(f32[768,2048]{1,0:T(8,128)S(1)} %fusion.18, bf16[768,384]{1,0:T(8,128)(2,1)S(1)} %get-tuple-element.16, bf16[1,2048,384]{2,1,0:T(8,128)(2,1)S(1)} %copy-done.4), kind=kOutput, calls=%fused_computation | convolution fusion | flops 1211105280 | bytes 11599872 | tf_op jit(solution)/shard_map/dot_general | solution.py:346
  79.7 26.4 %shard_map.182 = bf16[8,96,512]{2,1,0:T(8,128)(2,1)S(1)} custom-call(bf16[8,96,2048]{2,1,0:T(8,128)(2,1)S(1)} %bitcast.89), custom_call_target="tpu_custom_call" | custom-call | tf_op jit(solution)/shard_map/pallas_call | solution.py:321
  106.1 0.0 copy-start.5
  106.1 0.0 copy-start.10
  106.1 0.4 fusion.22
  106.5 0.4 copy-done.5
  106.9 0.1 convert_reduce_fusion
  107.0 0.2 fusion.54
  107.2 0.2 fusion.49.refs_1_
  107.4 16.2 %shard_map.183 = (bf16[4,64,2048]{2,1,0:T(8,128)(2,1)S(1)}, bf16[8,256,128]{2,1,0:T(8,128)(2,1)S(1)}) custom-call(bf16[4,64,512]{2,1,0:T(8,128)(2,1)S(1)} %bitcast.96, bf16[256,128]{1,0:T(8,128)(2,1)S(1)} %fusion.49.refs_1_), custom_call_target="tpu_custom_call" | custom-call | tf_op jit(solution)/shard_map/pallas_call | solution.py:207
  123.5 0.4 fusion.10
  124.0 0.0 copy-start.12
  124.0 0.7 fusion.9
  124.7 0.3 copy-done.12
  125.0 0.5 fusion.66
  125.6 0.2 fusion.53
  125.8 1.5 collective-permute-start
  127.3 3.0 %fusion = bf16[1,2048,384]{2,1,0:T(8,128)(2,1)} fusion(bf16[768,2048]{1,0:T(8,128)(2,1)S(1)} %bitcast.101, bf16[768,384]{1,0:T(8,128)(2,1)S(1)} %get-tuple-element.17), kind=kOutput, calls=%fused_computation.8 | convolution fusion | flops 1208745984 | bytes 5308416 | tf_op jit(solution)/shard_map/dot_general | solution.py:340
  130.3 3.0 %fusion.1 = bf16[1,2048,384]{2,1,0:T(8,128)(2,1)} fusion(bf16[768,2048]{1,0:T(8,128)(2,1)S(1)} %bitcast.102, bf16[768,384]{1,0:T(8,128)(2,1)S(1)} %get-tuple-element.16), kind=kOutput, calls=%fused_computation.9 | convolution fusion | flops 1208745984 | bytes 5308416 | tf_op jit(solution)/shard_map/dot_general | solution.py:340
  133.3 2.7 %fusion.2 = bf16[1,384,2048]{2,1,0:T(8,128)(2,1)} fusion(bf16[768,2048]{1,0:T(8,128)(2,1)S(1)} %bitcast.98, f32[768,384]{1,0:T(8,128)S(1)} %fusion.14, f32[768,384]{1,0:T(8,128)S(1)} %fusion.20), kind=kOutput, calls=%fused_computation.10 | convolution fusion | flops 1211695104 | bytes 7077888 | tf_op jit(solution)/shard_map/dot_general | solution.py:340
  136.0 1.0 constant_dynamic-slice_fusion.1
  137.0 0.9 constant_dynamic-slice_fusion
  137.9 0.0 copy-start.9
  138.0 22.9 %shard_map.184 = bf16[8,4,64,256]{3,2,1,0:T(8,128)(2,1)S(1)} custom-call(bf16[8,64,256]{2,1,0:T(8,128)(2,1)S(1)} %bitcast.93, bf16[4,64,256]{2,1,0:T(8,128)(2,1)S(1)} %bitcast.95), custom_call_target="tpu_custom_call" | custom-call | tf_op jit(solution)/shard_map/pallas_call | solution.py:207
  160.8 0.0 copy-start.13
  160.8 1.1 fusion.67
  162.0 0.0 collective-permute-done
  162.1 0.0 copy-done.13
  162.1 0.0 copy-start.7
  162.1 0.0 copy-start.8
  162.1 0.3 convolution_select_fusion
  162.5 0.4 copy-done.7
  162.9 0.0 copy-done.8
  163.0 0.7 multiply_convert_fusion.3
  (22 shorter events, 0.2 us)
Async XLA Ops:
  0.6 71.1 %copy-start = (bf16[1,2048,384]{2,1,0:T(8,128)(2,1)S(1)}, bf16[1,2048,384]{2,1,0:T(8,128)(2,1)}, u32[]{:S(2)}) copy-start(bf16[1,2048,384]{2,1,0:T(8,128)(2,1)} %param.19) | copy-start | bytes 4718596
  0.6 4.0 %copy-start.1 = (bf16[256,2048]{1,0:T(8,128)(2,1)S(1)}, bf16[256,2048]{1,0:T(8,128)(2,1)}, u32[]{:S(2)}) copy-start(bf16[256,2048]{1,0:T(8,128)(2,1)} %param.15) | copy-start | bytes 3145732
  0.7 4.0 %copy-start.6 = (f32[2048]{0:T(1024)S(1)}, f32[2048]{0:T(1024)}, u32[]{:S(2)}) copy-start(f32[2048]{0:T(1024)} %param.16) | copy-start | bytes 24580
  5.9 3.0 %copy-start.2 = (bf16[256,2048]{1,0:T(8,128)(2,1)S(1)}, bf16[256,2048]{1,0:T(8,128)(2,1)}, u32[]{:S(2)}) copy-start(bf16[256,2048]{1,0:T(8,128)(2,1)} %param.14) | copy-start | bytes 3145732
  9.3 60.6 %copy-start.4 = (bf16[1,2048,384]{2,1,0:T(8,128)(2,1)S(1)}, bf16[1,2048,384]{2,1,0:T(8,128)(2,1)}, u32[]{:S(2)}) copy-start(bf16[1,2048,384]{2,1,0:T(8,128)(2,1)} %param.20) | copy-start | bytes 4718596
  71.7 1.8 %copy-start.11 = (bf16[1,384,2048]{2,1,0:T(8,128)(2,1)S(1)}, bf16[1,384,2048]{2,1,0:T(8,128)(2,1)}, u32[]{:S(2)}) copy-start(bf16[1,384,2048]{2,1,0:T(8,128)(2,1)} %param.21) | copy-start | bytes 4718596
  106.1 0.8 copy-start.5
  106.1 1.1 copy-start.10
  124.0 1.0 copy-start.12
  125.0 5.3 %copy-start.3 = (bf16[256,2048]{1,0:T(8,128)(2,1)}, bf16[256,2048]{1,0:T(8,128)(2,1)S(1)}, u32[]{:S(2)}) copy-start(bf16[256,2048]{1,0:T(8,128)(2,1)S(1)} %fusion.9) | copy-start | bytes 3145732
  125.8 36.2 %collective-permute-start = (f32[30,128]{1,0:T(8,128)S(1)}, f32[30,128]{1,0:T(8,128)S(1)}, u32[]{:S(2)}, u32[]{:S(2)}) collective-permute-start(f32[30,128]{1,0:T(8,128)S(1)} %slice.22), channel_id=1, source_target_pairs={{4,0},{8,4},{12,8},{16,12},{20,16},{24,20},{28,24},{5,1},{9,5},{13... | collective-permute-start | bytes 46088 | tf_op jit(solution)/shard_map/ppermute | solution.py:22
  137.9 24.0 %copy-start.9 = (f32[31,128]{1,0:T(8,128)S(1)}, f32[31,128]{1,0:T(8,128)}, u32[]{:S(2)}) copy-start(f32[31,128]{1,0:T(8,128)} %param.25) | copy-start | bytes 47620
  160.8 1.3 copy-start.13
  162.1 0.8 copy-start.7
  162.1 0.9 copy-start.8
